TPU v7x, 32 devices: a whole 2x2x4 slice. The times are simulated.
32 devices in a mesh: kv: 8 (over z, y), tp: 4 (over x, core).
Axes of the slice: x: 2, y: 2, z: 4, core: 2. Of those that a mesh axis runs over, the one named last changes fastest.
Arguments:
- tokens: bfloat16 [8192, 1024], P('kv', 'tp'), may hold values from -6 to 6
- query_weight: bfloat16 [1024, 2048], P(None, 'tp'), may hold values from -0.1875 to 0.1875
- latent_weight: bfloat16 [1024, 128], replicated, may hold values from -0.1875 to 0.1875
- query_gain: float32 [128], replicated, may hold values from 0.5 to 1.5
- key_gain: float32 [128], replicated, may hold values from 0.5 to 1.5
- value_up: bfloat16 [16, 128, 64], P('tp'), may hold values from -0.5 to 0.5
- out_weight: bfloat16 [1024, 1024], P('tp'), may hold values from -0.25 to 0.25
- out_gain: float32 [1024], replicated, may hold values from 0.5 to 1.5
- chosen: int32 [64, 32], P('kv'), may hold values from -1 to 63, as said below
Outputs:
- mixed_out: bfloat16 [8192, 1024], P('kv', 'tp')
Inputs may be any that keep to these rules, and one draw needn't show every extreme that they name: Row b lists the key blocks chosen for query block b: entry 0 is b itself, then distinct blocks before b, then -1 in every unused place. Block j is held by index j // 8 of kv. All query blocks of one index of kv together choose at most 2 distinct blocks held by any one other index, and some pair of indices reaches that bound; blocks held by the same index are chosen freely.
All inputs are finite; a program needn't handle non-finite values.
Results may differ from a plain program's by a relative error of at most 0.02.
Values may be sent and summed in bfloat16 or wider, within the bound.
A program may use at most 64 MiB of HBM per device.

v0:
```python
import jax
import jax.numpy as jnp
from jax import lax
from jax.sharding import PartitionSpec as P

BLOCK = 128
PER_OWNER = 2
epsilon = 1e-06
masked_score = -1e30


def taken_in(shard, axis, dim, absorb, carry):
    whole = jax.tree.map(lambda part: lax.all_gather(part, axis, axis=dim, tiled=True), shard)
    return absorb(carry, whole, jnp.int32(0))


def own_rows(product, rows, axis):
    everything = product(jnp.int32(0), lax.axis_size(axis) * rows)
    own = lax.psum_scatter(everything.astype(jnp.bfloat16), axis, scatter_dimension=0, tiled=True)
    return own.astype(jnp.float32)


def rms_scale(values, gain_row):
    widened = values.astype(jnp.float32)
    mean_sq = jnp.mean(widened * widened, axis=-1, keepdims=True)
    return (widened * lax.rsqrt(mean_sq + epsilon) * gain_row).astype(jnp.bfloat16)


def on_device(
    tokens,
    query_weight,
    latent_weight,
    query_gain,
    key_gain,
    value_up,
    out_weight,
    out_gain,
    chosen,
):
    tok_rows = tokens.shape[0]
    head_cols = query_weight.shape[1]
    lat_width = latent_weight.shape[1]
    local_heads = head_cols // lat_width
    block_size = BLOCK
    blocks_dev = tok_rows // block_size
    owners = lax.axis_size("kv")
    my_owner = lax.axis_index("kv")

    def project(totals, shard_piece, offset):
        query_rows = lax.dynamic_slice_in_dim(query_weight, offset, shard_piece.shape[1], 0)
        latent_rows = lax.dynamic_slice_in_dim(latent_weight, offset, shard_piece.shape[1], 0)
        return (
            totals[0] + jnp.dot(shard_piece, query_rows, preferred_element_type=jnp.float32),
            totals[1] + jnp.dot(shard_piece, latent_rows, preferred_element_type=jnp.float32),
        )

    query_zero = jnp.zeros((tok_rows, head_cols), jnp.float32)
    latent_zero = jnp.zeros((tok_rows, lat_width), jnp.float32)
    query_acc, latent_acc = taken_in(tokens, "tp", 1, project, (query_zero, latent_zero))
    queries = rms_scale(
        query_acc.astype(jnp.bfloat16).reshape(tok_rows, local_heads, lat_width), query_gain
    )
    latent = latent_acc.astype(jnp.bfloat16)
    latent_blocks = latent.reshape(blocks_dev, block_size, lat_width)
    clamped = jnp.maximum(chosen, 0)
    owner_of = clamped // blocks_dev
    index_in = clamped % blocks_dev
    flat_owner = owner_of.reshape(-1)
    flat_index = index_in.reshape(-1)
    remote = (chosen.reshape(-1) >= 0) & (flat_owner != my_owner)
    owner_ids = jnp.arange(owners, dtype=jnp.int32)
    local_ids = jnp.arange(blocks_dev, dtype=jnp.int32)
    matches = (
        remote[:, None, None]
        & (flat_owner[:, None, None] == owner_ids[None, :, None])
        & (flat_index[:, None, None] == local_ids[None, None, :])
    )
    needed = jnp.any(matches, axis=0)
    ranking = jnp.cumsum(needed.astype(jnp.int32), axis=1) - 1
    slot_ids = jnp.arange(PER_OWNER, dtype=jnp.int32)
    placed = needed[:, None, :] & (ranking[:, None, :] == slot_ids[None, :, None])
    wanted = jnp.where(
        jnp.any(placed, axis=2), jnp.sum(jnp.where(placed, local_ids[None, None, :], 0), axis=2), -1
    )
    requested = lax.all_to_all(wanted, "kv", split_axis=0, concat_axis=0, tiled=True)
    served = latent_blocks[jnp.maximum(requested, 0)]
    served = jnp.where((requested >= 0)[:, :, None, None], served, jnp.zeros_like(served))
    arrived = lax.all_to_all(served, "kv", split_axis=0, concat_axis=0, tiled=True)
    block_pool = jnp.concatenate(
        [latent_blocks, arrived.reshape(owners * PER_OWNER, block_size, lat_width)], axis=0
    )
    slot_of = jnp.sum(jnp.where(wanted[owner_of] == index_in[:, :, None], slot_ids, 0), axis=2)
    where_from = jnp.where(
        owner_of == my_owner, index_in, blocks_dev + owner_of * PER_OWNER + slot_of
    )
    selected = block_pool[where_from]
    score_scale = lat_width ** (-0.5)
    offsets = jnp.arange(block_size, dtype=jnp.int32)
    query_blocks = queries.reshape(blocks_dev, block_size, local_heads, lat_width)
    block_starts = my_owner * tok_rows + jnp.arange(blocks_dev, dtype=jnp.int32) * block_size

    def attend(packed):
        query_block, picked_values, chosen_row, start_pos = packed
        picked_keys = rms_scale(picked_values, key_gain)
        scores = (
            jnp.einsum(
                "qhl,ckl->qhck", query_block, picked_keys, preferred_element_type=jnp.float32
            )
            * score_scale
        )
        key_pos = jnp.maximum(chosen_row, 0)[:, None] * block_size + offsets[None, :]
        query_pos = start_pos + offsets
        allowed = (chosen_row[:, None] >= 0)[None] & (key_pos[None] <= query_pos[:, None, None])
        allowed = allowed[:, None]
        scores = jnp.where(allowed, scores, masked_score)
        row_max = jnp.max(scores, axis=(2, 3), keepdims=True)
        exp_scores = jnp.where(allowed, jnp.exp(scores - row_max), 0.0)
        weights = (exp_scores / jnp.sum(exp_scores, axis=(2, 3), keepdims=True)).astype(
            jnp.bfloat16
        )
        attended = jnp.einsum(
            "qhck,ckl->qhl", weights, picked_values, preferred_element_type=jnp.float32
        )
        return attended.astype(jnp.bfloat16)

    attended = lax.map(attend, (query_blocks, selected, chosen, block_starts))
    attended = attended.reshape(tok_rows, local_heads, lat_width)
    heads_out = jnp.einsum("thl,hlv->thv", attended, value_up, preferred_element_type=jnp.float32)
    heads_out = heads_out.astype(jnp.bfloat16).reshape(tok_rows, local_heads * value_up.shape[2])
    model_width = out_weight.shape[1]
    tp_count = lax.axis_size("tp")
    feature_rows = model_width // tp_count
    gain_part = lax.dynamic_slice_in_dim(
        out_gain, lax.axis_index("tp") * feature_rows, feature_rows, 0
    )

    def columns(offset, count):
        weight_cols = lax.dynamic_slice_in_dim(out_weight, offset, count, 1)
        return lax.dot_general(
            weight_cols, heads_out, (((0,), (1,)), ((), ())), preferred_element_type=jnp.float32
        )

    summed = own_rows(columns, feature_rows, "tp").T
    squares = lax.psum(jnp.sum(summed * summed, axis=1), "tp")
    mixed_out = (summed * lax.rsqrt(squares / model_width + epsilon)[:, None] * gain_part).astype(
        jnp.bfloat16
    )
    return mixed_out


def solution(mesh):
    in_specs = (
        P("kv", "tp"),
        P(None, "tp"),
        P(),
        P(),
        P(),
        P("tp", None, None),
        P("tp", None),
        P(),
        P("kv", None),
    )
    out_specs = P("kv", "tp")
    return jax.shard_map(
        on_device, mesh=mesh, in_specs=in_specs, out_specs=out_specs, check_vma=False
    )
```

profile of v0, /device:TPU:0, one launch (start us, length us, event | category | flops | bytes accessed | tf_op | source)
XLA Modules:
  0.0 234.5 jit_solution(9330237730256950675)
XLA Ops:
  10.4 7.3 %all-to-all-start = ((s32[8,1,2]{2,1,0:T(1,128)}), s32[8,1,2]{2,1,0:T(1,128)S(1)}, u32[]{:S(2)}, u32[]{:S(2)}) async-start(s32[8,1,2]{2,1,0:T(1,128)} %bitcast.27), calls=%async_computation | async-start | bytes 8192 | tf_op jit(solution)/shard_map/all_to_all | solution.py:85
  20.3 3.8 %all-to-all-done = s32[8,1,2]{2,1,0:T(1,128)S(1)} async-done(((s32[8,1,2]{2,1,0:T(1,128)}), s32[8,1,2]{2,1,0:T(1,128)S(1)}, u32[]{:S(2)}, u32[]{:S(2)}) %all-to-all-start) | async-done | bytes 96 | tf_op jit(solution)/shard_map/all_to_all | solution.py:85
  24.5 10.0 %all-gather.2.cloned.1.call-done = bf16[1024,1024]{1,0:T(8,128)(2,1)} async-done(((bf16[1024,256]{1,0:T(8,128)(2,1)}), bf16[1024,1024]{1,0:T(8,128)(2,1)}) %all-gather.2.cloned.1.call-update) | async-done | bytes 2097168 | tf_op jit(solution)/shard_map/all_gather | solution.py:13
  34.5 2.3 convolution_convert_fusion.2
  38.3 5.5 %all-to-all-start.1 = ((bf16[8,2,128,128]{3,2,1,0:T(8,128)(2,1)}), bf16[8,2,128,128]{3,2,1,0:T(8,128)(2,1)}, u32[]{:S(2)}, u32[]{:S(2)}) async-start(bf16[8,2,128,128]{3,2,1,0:T(8,128)(2,1)} %broadcast_select_fusion), calls=%async_computation.1 | async-start | bytes 1048576 | tf_op jit(solution)/shard_map/all_to_all | solution.py:88
  43.9 2.9 %bitcast_reduce_fusion = (f32[1024,4]{0,1:T(4,128)S(1)}, bf16[1024,512]{0,1:T(8,128)(2,1)S(1)}) fusion(bf16[1024,1024]{1,0:T(8,128)(2,1)} %all-gather.2.cloned.1.call-done, bf16[1024,512]{1,0:T(8,128)(2,1)S(1)} %copy-done), kind=kOutput, calls=%fused_computation.39 | convolution fusion | flops 1075834880 | bytes 4210688 | tf_op jit(solution)/shard_map/dot_general | solution.py:53
  52.4 6.4 %all-to-all-done.1 = bf16[8,2,128,128]{3,2,1,0:T(8,128)(2,1)} async-done(((bf16[8,2,128,128]{3,2,1,0:T(8,128)(2,1)}), bf16[8,2,128,128]{3,2,1,0:T(8,128)(2,1)}, u32[]{:S(2)}, u32[]{:S(2)}) %all-to-all-start.1) | async-done | bytes 524320 | tf_op jit(solution)/shard_map/all_to_all | solution.py:88
  60.0 8.3 %gather_fusion.2 = bf16[256,128,128]{2,1,0:T(8,128)(2,1)} fusion(bf16[24,128,128]{2,1,0:T(8,128)(2,1)S(1)} %pad_maximum_fusion, s32[1024]{0:T(1024)S(1)} %pad_clamp_fusion), kind=kCustom, calls=%fused_computation.2 | custom fusion | bytes 16778240 | tf_op jit(solution)/shard_map/gather | solution.py:96
  68.3 118.1 %while.12 = (s32[]{:T(128)}, bf16[8,128,4,128]{3,1,0,2:T(8,128)(2,1)S(1)}, s32[8,32]{1,0:T(8,128)}, s32[8]{0:T(128)S(1)}, bf16[8,128,4,128]{3,1,2,0:T(8,128)(2,1...) while((s32[]{:T(128)}, ...), condition=%wide.region_10.11_spmd.clone.clone, body=%wide.region_6.10_spmd.clone.clone.sunk | while | flops 1107893504 | bytes 30783664 | solution.py:126
  73.7 2.8 %fusion.45 = (f32[128,4]{0,1:T(4,128)S(1)}, f32[128,4,32,128]{0,3,2,1:T(8,128)S(1)}) fusion(pred[128,32,128]{0,2,1:T(8,128)(4,1)S(1)} %compare_and_fusion.3, f32[128]{0:T(128)S(1)} %get-tuple-element.179, f32[32,128]{1,0:T(8,128)S(1)} %add_rsqrt_fusion.3, bf16[8,32,128,128]{3,2,1,0:T(8,128)(2,1)} %get-tuple-element.178, s32[]{:T(128)} %get-tuple-element.165, ...), kind=kOutput, calls=%fused_computation.7.clone.1 | convolution fusion | flops 545259008 | bytes 10112512 | tf_op jit(solution)/shard_map/while/body/eval_jaxpr/qhl,ckl->qhck/dot_general | solution.py:106
  76.5 2.1 fusion.46
  78.6 4.5 %fusion.47 = bf16[8,128,4,128]{3,1,0,2:T(8,128)(2,1)S(1)} fusion(bf16[8,128,4,128]{3,1,0,2:T(8,128)(2,1)S(1)} %get-tuple-element.166, s32[]{:T(128)} %get-tuple-element.165, f32[128,4,32,128]{0,3,2,1:T(8,128)S(1)} %get-tuple-element.155, f32[128,4]{0,1:T(4,128)S(1)} %fusion.46, f32[128,4]{0,1:T(4,128)S(1)} %get-tuple-element.156, ...), kind=kOutput, calls=%fused_computation.16.clone.1 | convolution fusion | flops 549519360 | bytes 10097664 | tf_op jit(solution)/shard_map/while/body/eval_jaxpr/qhck,ckl->qhl/dot_general | solution.py:121
  88.5 2.8 %fusion.45 = (f32[128,4]{0,1:T(4,128)S(1)}, f32[128,4,32,128]{0,3,2,1:T(8,128)S(1)}) fusion(pred[128,32,128]{0,2,1:T(8,128)(4,1)S(1)} %compare_and_fusion.3, f32[128]{0:T(128)S(1)} %get-tuple-element.179, f32[32,128]{1,0:T(8,128)S(1)} %add_rsqrt_fusion.3, bf16[8,32,128,128]{3,2,1,0:T(8,128)(2,1)} %get-tuple-element.178, s32[]{:T(128)} %get-tuple-element.165, ...), kind=kOutput, calls=%fused_computation.7.clone.1 | convolution fusion | flops 545259008 | bytes 10112512 | tf_op jit(solution)/shard_map/while/body/eval_jaxpr/qhl,ckl->qhck/dot_general | solution.py:106
  91.3 2.1 fusion.46
  93.4 4.5 %fusion.47 = bf16[8,128,4,128]{3,1,0,2:T(8,128)(2,1)S(1)} fusion(bf16[8,128,4,128]{3,1,0,2:T(8,128)(2,1)S(1)} %get-tuple-element.166, s32[]{:T(128)} %get-tuple-element.165, f32[128,4,32,128]{0,3,2,1:T(8,128)S(1)} %get-tuple-element.155, f32[128,4]{0,1:T(4,128)S(1)} %fusion.46, f32[128,4]{0,1:T(4,128)S(1)} %get-tuple-element.156, ...), kind=kOutput, calls=%fused_computation.16.clone.1 | convolution fusion | flops 549519360 | bytes 10097664 | tf_op jit(solution)/shard_map/while/body/eval_jaxpr/qhck,ckl->qhl/dot_general | solution.py:121
  103.3 2.8 %fusion.45 = (f32[128,4]{0,1:T(4,128)S(1)}, f32[128,4,32,128]{0,3,2,1:T(8,128)S(1)}) fusion(pred[128,32,128]{0,2,1:T(8,128)(4,1)S(1)} %compare_and_fusion.3, f32[128]{0:T(128)S(1)} %get-tuple-element.179, f32[32,128]{1,0:T(8,128)S(1)} %add_rsqrt_fusion.3, bf16[8,32,128,128]{3,2,1,0:T(8,128)(2,1)} %get-tuple-element.178, s32[]{:T(128)} %get-tuple-element.165, ...), kind=kOutput, calls=%fused_computation.7.clone.1 | convolution fusion | flops 545259008 | bytes 10112512 | tf_op jit(solution)/shard_map/while/body/eval_jaxpr/qhl,ckl->qhck/dot_general | solution.py:106
  106.0 2.1 fusion.46
  108.1 4.5 %fusion.47 = bf16[8,128,4,128]{3,1,0,2:T(8,128)(2,1)S(1)} fusion(bf16[8,128,4,128]{3,1,0,2:T(8,128)(2,1)S(1)} %get-tuple-element.166, s32[]{:T(128)} %get-tuple-element.165, f32[128,4,32,128]{0,3,2,1:T(8,128)S(1)} %get-tuple-element.155, f32[128,4]{0,1:T(4,128)S(1)} %fusion.46, f32[128,4]{0,1:T(4,128)S(1)} %get-tuple-element.156, ...), kind=kOutput, calls=%fused_computation.16.clone.1 | convolution fusion | flops 549519360 | bytes 10097664 | tf_op jit(solution)/shard_map/while/body/eval_jaxpr/qhck,ckl->qhl/dot_general | solution.py:121
  118.0 2.8 %fusion.45 = (f32[128,4]{0,1:T(4,128)S(1)}, f32[128,4,32,128]{0,3,2,1:T(8,128)S(1)}) fusion(pred[128,32,128]{0,2,1:T(8,128)(4,1)S(1)} %compare_and_fusion.3, f32[128]{0:T(128)S(1)} %get-tuple-element.179, f32[32,128]{1,0:T(8,128)S(1)} %add_rsqrt_fusion.3, bf16[8,32,128,128]{3,2,1,0:T(8,128)(2,1)} %get-tuple-element.178, s32[]{:T(128)} %get-tuple-element.165, ...), kind=kOutput, calls=%fused_computation.7.clone.1 | convolution fusion | flops 545259008 | bytes 10112512 | tf_op jit(solution)/shard_map/while/body/eval_jaxpr/qhl,ckl->qhck/dot_general | solution.py:106
  120.8 2.1 fusion.46
  122.9 4.5 %fusion.47 = bf16[8,128,4,128]{3,1,0,2:T(8,128)(2,1)S(1)} fusion(bf16[8,128,4,128]{3,1,0,2:T(8,128)(2,1)S(1)} %get-tuple-element.166, s32[]{:T(128)} %get-tuple-element.165, f32[128,4,32,128]{0,3,2,1:T(8,128)S(1)} %get-tuple-element.155, f32[128,4]{0,1:T(4,128)S(1)} %fusion.46, f32[128,4]{0,1:T(4,128)S(1)} %get-tuple-element.156, ...), kind=kOutput, calls=%fused_computation.16.clone.1 | convolution fusion | flops 549519360 | bytes 10097664 | tf_op jit(solution)/shard_map/while/body/eval_jaxpr/qhck,ckl->qhl/dot_general | solution.py:121
  132.8 2.8 %fusion.45 = (f32[128,4]{0,1:T(4,128)S(1)}, f32[128,4,32,128]{0,3,2,1:T(8,128)S(1)}) fusion(pred[128,32,128]{0,2,1:T(8,128)(4,1)S(1)} %compare_and_fusion.3, f32[128]{0:T(128)S(1)} %get-tuple-element.179, f32[32,128]{1,0:T(8,128)S(1)} %add_rsqrt_fusion.3, bf16[8,32,128,128]{3,2,1,0:T(8,128)(2,1)} %get-tuple-element.178, s32[]{:T(128)} %get-tuple-element.165, ...), kind=kOutput, calls=%fused_computation.7.clone.1 | convolution fusion | flops 545259008 | bytes 10112512 | tf_op jit(solution)/shard_map/while/body/eval_jaxpr/qhl,ckl->qhck/dot_general | solution.py:106
  137.7 4.5 %fusion.47 = bf16[8,128,4,128]{3,1,0,2:T(8,128)(2,1)S(1)} fusion(bf16[8,128,4,128]{3,1,0,2:T(8,128)(2,1)S(1)} %get-tuple-element.166, s32[]{:T(128)} %get-tuple-element.165, f32[128,4,32,128]{0,3,2,1:T(8,128)S(1)} %get-tuple-element.155, f32[128,4]{0,1:T(4,128)S(1)} %fusion.46, f32[128,4]{0,1:T(4,128)S(1)} %get-tuple-element.156, ...), kind=kOutput, calls=%fused_computation.16.clone.1 | convolution fusion | flops 549519360 | bytes 10097664 | tf_op jit(solution)/shard_map/while/body/eval_jaxpr/qhck,ckl->qhl/dot_general | solution.py:121
  147.5 2.8 %fusion.45 = (f32[128,4]{0,1:T(4,128)S(1)}, f32[128,4,32,128]{0,3,2,1:T(8,128)S(1)}) fusion(pred[128,32,128]{0,2,1:T(8,128)(4,1)S(1)} %compare_and_fusion.3, f32[128]{0:T(128)S(1)} %get-tuple-element.179, f32[32,128]{1,0:T(8,128)S(1)} %add_rsqrt_fusion.3, bf16[8,32,128,128]{3,2,1,0:T(8,128)(2,1)} %get-tuple-element.178, s32[]{:T(128)} %get-tuple-element.165, ...), kind=kOutput, calls=%fused_computation.7.clone.1 | convolution fusion | flops 545259008 | bytes 10112512 | tf_op jit(solution)/shard_map/while/body/eval_jaxpr/qhl,ckl->qhck/dot_general | solution.py:106
  152.4 4.5 %fusion.47 = bf16[8,128,4,128]{3,1,0,2:T(8,128)(2,1)S(1)} fusion(bf16[8,128,4,128]{3,1,0,2:T(8,128)(2,1)S(1)} %get-tuple-element.166, s32[]{:T(128)} %get-tuple-element.165, f32[128,4,32,128]{0,3,2,1:T(8,128)S(1)} %get-tuple-element.155, f32[128,4]{0,1:T(4,128)S(1)} %fusion.46, f32[128,4]{0,1:T(4,128)S(1)} %get-tuple-element.156, ...), kind=kOutput, calls=%fused_computation.16.clone.1 | convolution fusion | flops 549519360 | bytes 10097664 | tf_op jit(solution)/shard_map/while/body/eval_jaxpr/qhck,ckl->qhl/dot_general | solution.py:121
  162.3 2.8 %fusion.45 = (f32[128,4]{0,1:T(4,128)S(1)}, f32[128,4,32,128]{0,3,2,1:T(8,128)S(1)}) fusion(pred[128,32,128]{0,2,1:T(8,128)(4,1)S(1)} %compare_and_fusion.3, f32[128]{0:T(128)S(1)} %get-tuple-element.179, f32[32,128]{1,0:T(8,128)S(1)} %add_rsqrt_fusion.3, bf16[8,32,128,128]{3,2,1,0:T(8,128)(2,1)} %get-tuple-element.178, s32[]{:T(128)} %get-tuple-element.165, ...), kind=kOutput, calls=%fused_computation.7.clone.1 | convolution fusion | flops 545259008 | bytes 10112512 | tf_op jit(solution)/shard_map/while/body/eval_jaxpr/qhl,ckl->qhck/dot_general | solution.py:106
  167.2 4.5 %fusion.47 = bf16[8,128,4,128]{3,1,0,2:T(8,128)(2,1)S(1)} fusion(bf16[8,128,4,128]{3,1,0,2:T(8,128)(2,1)S(1)} %get-tuple-element.166, s32[]{:T(128)} %get-tuple-element.165, f32[128,4,32,128]{0,3,2,1:T(8,128)S(1)} %get-tuple-element.155, f32[128,4]{0,1:T(4,128)S(1)} %fusion.46, f32[128,4]{0,1:T(4,128)S(1)} %get-tuple-element.156, ...), kind=kOutput, calls=%fused_computation.16.clone.1 | convolution fusion | flops 549519360 | bytes 10097664 | tf_op jit(solution)/shard_map/while/body/eval_jaxpr/qhck,ckl->qhl/dot_general | solution.py:121
  177.1 2.8 %fusion.45 = (f32[128,4]{0,1:T(4,128)S(1)}, f32[128,4,32,128]{0,3,2,1:T(8,128)S(1)}) fusion(pred[128,32,128]{0,2,1:T(8,128)(4,1)S(1)} %compare_and_fusion.3, f32[128]{0:T(128)S(1)} %get-tuple-element.179, f32[32,128]{1,0:T(8,128)S(1)} %add_rsqrt_fusion.3, bf16[8,32,128,128]{3,2,1,0:T(8,128)(2,1)} %get-tuple-element.178, s32[]{:T(128)} %get-tuple-element.165, ...), kind=kOutput, calls=%fused_computation.7.clone.1 | convolution fusion | flops 545259008 | bytes 10112512 | tf_op jit(solution)/shard_map/while/body/eval_jaxpr/qhl,ckl->qhck/dot_general | solution.py:106
  182.0 4.5 %fusion.47 = bf16[8,128,4,128]{3,1,0,2:T(8,128)(2,1)S(1)} fusion(bf16[8,128,4,128]{3,1,0,2:T(8,128)(2,1)S(1)} %get-tuple-element.166, s32[]{:T(128)} %get-tuple-element.165, f32[128,4,32,128]{0,3,2,1:T(8,128)S(1)} %get-tuple-element.155, f32[128,4]{0,1:T(4,128)S(1)} %fusion.46, f32[128,4]{0,1:T(4,128)S(1)} %get-tuple-element.156, ...), kind=kOutput, calls=%fused_computation.16.clone.1 | convolution fusion | flops 549519360 | bytes 10097664 | tf_op jit(solution)/shard_map/while/body/eval_jaxpr/qhck,ckl->qhl/dot_general | solution.py:121
  187.0 2.1 convert_bitcast_fusion.1
  189.9 28.7 %reduce-scatter.2.cloned.1.call-done = bf16[256,1024]{0,1:T(8,128)(2,1)} async-done(((bf16[1024,1024]{0,1:T(8,128)(2,1)}), bf16[256,1024]{0,1:T(8,128)(2,1)}) %reduce-scatter.2.cloned.1.call-update) | async-done | bytes 524304 | tf_op jit(solution)/shard_map/reduce_scatter | solution.py:19
  219.8 5.8 %psum.7 = f32[1024]{0:T(1024)S(1)} all-reduce(f32[1024]{0:T(1024)S(1)} %fusion.24), channel_id=1, replica_groups=mesh['kv'=8,'tp'=4] {'tp'}, use_global_device_ids=true, to_apply=%region_13.14 | all-reduce | flops 1024 | bytes 8192 | tf_op jit(solution)/shard_map/psum | solution.py:144
  (128 shorter events, 70.7 us)
Async XLA Ops:
  6.5 37.4 %copy-start = (bf16[1024,512]{1,0:T(8,128)(2,1)S(1)}, bf16[1024,512]{1,0:T(8,128)(2,1)}, u32[]{:S(2)}) copy-start(bf16[1024,512]{1,0:T(8,128)(2,1)} %param.12) | copy-start | bytes 3145732
  6.5 27.9 %all-gather.2.cloned.1.call-start = ((), (), s32[]{:S(2)}) async-start(), calls=%async_computation.3 | async-start | bytes 2621440 | tf_op jit(solution)/shard_map/all_gather | solution.py:13
  10.4 13.7 %all-to-all-start = ((s32[8,1,2]{2,1,0:T(1,128)}), s32[8,1,2]{2,1,0:T(1,128)S(1)}, u32[]{:S(2)}, u32[]{:S(2)}) async-start(s32[8,1,2]{2,1,0:T(1,128)} %bitcast.27), calls=%async_computation | async-start | bytes 8192 | tf_op jit(solution)/shard_map/all_to_all | solution.py:85
  38.3 20.5 %all-to-all-start.1 = ((bf16[8,2,128,128]{3,2,1,0:T(8,128)(2,1)}), bf16[8,2,128,128]{3,2,1,0:T(8,128)(2,1)}, u32[]{:S(2)}, u32[]{:S(2)}) async-start(bf16[8,2,128,128]{3,2,1,0:T(8,128)(2,1)} %broadcast_select_fusion), calls=%async_computation.1 | async-start | bytes 1048576 | tf_op jit(solution)/shard_map/all_to_all | solution.py:88
  43.8 7.0 %copy-start.4 = (f32[128]{0:T(128)S(1)}, f32[128]{0:T(128)}, u32[]{:S(2)}) copy-start(f32[128]{0:T(128)} %param.14) | copy-start | bytes 1540
  43.9 174.7 %reduce-scatter.2.cloned.1.call-start = ((), (), s32[]{:S(2)}) async-start(), calls=%async_computation.4 | async-start | bytes 2621440 | tf_op jit(solution)/shard_map/reduce_scatter | solution.py:19
  60.0 8.3 %copy-start.1 = (bf16[8,128,4,128]{3,1,0,2:T(8,128)(2,1)S(1)}, bf16[8,128,4,128]{3,1,0,2:T(8,128)(2,1)}, u32[]{:S(2)}) copy-start(bf16[8,128,4,128]{3,1,0,2:T(8,128)(2,1)} %custom-call.6) | copy-start | bytes 3145732
  60.0 8.3 %copy-start.5 = (f32[128]{0:T(128)S(1)}, f32[128]{0:T(128)}, u32[]{:S(2)}) copy-start(f32[128]{0:T(128)} %param.15) | copy-start | bytes 1540
  68.3 118.2 %copy-start.3 = (bf16[4,128,64]{1,2,0:T(8,128)(2,1)S(1)}, bf16[4,128,64]{1,2,0:T(8,128)(2,1)}, u32[]{:S(2)}) copy-start(bf16[4,128,64]{1,2,0:T(8,128)(2,1)} %param.16) | copy-start | bytes 196612
  68.3 118.7 %copy-start.2 = (bf16[256,1024]{1,0:T(8,128)(2,1)S(1)}, bf16[256,1024]{1,0:T(8,128)(2,1)}, u32[]{:S(2)}) copy-start(bf16[256,1024]{1,0:T(8,128)(2,1)} %param.17) | copy-start | bytes 1572868
Sparse Core Ops, SparseCore 0:
  8.9 25.5 all-gather.1
  189.2 29.3 reduce-scatter.1
where the time goes:
time: 236 us; the launch traced here: 234 us
  matrix products  66 us (28%)
  other arithmetic  65.6 us (28%)
  waiting for transfers between devices  49.7 us (21%)
  local copies, waits for them, and re-layouts  20.4 us (9%)
  between operations  13.6 us (6%)
  starting transfers between devices  12.9 us (5%)
  blocking collectives  5.77 us (2%)
    dot_general x8, matrix products, attend(): jnp.einsum('qhck,ckl->qhl', weights, picked_values, preferred_element_typ...  35.9 us
    reduce_scatter x1, waiting for transfers between devices, own_rows(): lax.psum_scatter(everything.astype(jnp.bfloat16), axis, scatter_dimension...  28.7 us
    dot_general x8, matrix products, attend(): jnp.einsum('qhl,ckl->qhck', query_block, picked_keys, preferred_element_t...  22.3 us
    reduce_sum x8, other arithmetic, attend(): jnp.sum(exp_scores, axis=(2, 3), keepdims=True)  16.7 us
    reduce_sum x8, other arithmetic, rms_scale(): mean_sq = jnp.mean(widened * widened, axis=-1, keepdims=True)  14.7 us
    all_gather x1, waiting for transfers between devices, taken_in(): lax.all_gather(part, axis, axis=dim, tiled=True)  9.99 us
    gather x1, local copies, waits for them, and re-layouts, on_device(): selected = block_pool[where_from]  8.29 us
    all_to_all x1, starting transfers between devices, on_device(): lax.all_to_all(wanted, 'kv', split_axis=0, concat_axis=0, tiled=True)  7.31 us
  transfers between devices with their start and end apart: 4, of which 4 were waited for; matrix products, arithmetic and copies ran while one was open for 7% of the time, Pallas kernels for 0%

commit v1 on v0

--- a/solution.py
+++ b/solution.py
@@ -7,6 +7,22 @@
 PER_OWNER = 2
 epsilon = 1e-06
 masked_score = -1e30
+
+
+def pairwise_exchange(x, axis, split, join):
+    ways, here = (lax.axis_size(axis), lax.axis_index(axis))
+    width = x.shape[split] // ways
+    lengths = list(x.shape)
+    lengths[split] = width
+    height = lengths[join]
+    lengths[join] = height * ways
+    full = jnp.zeros(lengths, x.dtype)
+    for mask in range(ways):
+        part = lax.dynamic_slice_in_dim(x, (here ^ mask) * width, width, axis=split)
+        if mask:
+            part = lax.ppermute(part, axis, [(d, d ^ mask) for d in range(ways)])
+        full = lax.dynamic_update_slice_in_dim(full, part, (here ^ mask) * height, axis=join)
+    return full
 
 
 def taken_in(shard, axis, dim, absorb, carry):
@@ -85,7 +101,7 @@
     requested = lax.all_to_all(wanted, "kv", split_axis=0, concat_axis=0, tiled=True)
     served = latent_blocks[jnp.maximum(requested, 0)]
     served = jnp.where((requested >= 0)[:, :, None, None], served, jnp.zeros_like(served))
-    arrived = lax.all_to_all(served, "kv", split_axis=0, concat_axis=0, tiled=True)
+    arrived = pairwise_exchange(served, "kv", 0, 0)
     block_pool = jnp.concatenate(
         [latent_blocks, arrived.reshape(owners * PER_OWNER, block_size, lat_width)], axis=0
     )

time: 236 us -> 248 us (1.051)
  local copies, waits for them, and re-layouts: 20.4 us -> 30.7 us
  starting transfers between devices: 12.9 us -> 18.5 us
  waiting for transfers between devices: 49.7 us -> 45.1 us
    ppermute x0 -> x7, starting transfers between devices: none -> 11.1 us  [pairwise_exchange(): part = lax.ppermute(part, axis, [(d, d ^ mask) for d in range(ways)])]
    dynamic_update_slice x0 -> x7, local copies, waits for them, and re-layouts: none -> 8.63 us  [pairwise_exchange(): lax.dynamic_update_slice_in_dim(full, part, (here ^ mask) * height, axis=...]
    all_to_all x1 -> x0, waiting for transfers between devices: 6.42 us -> none  [on_device(): lax.all_to_all(served, 'kv', split_axis=0, concat_axis=0, tiled=True)]
    all_to_all x1 -> x0, starting transfers between devices: 5.54 us -> none  [on_device(): lax.all_to_all(served, 'kv', split_axis=0, concat_axis=0, tiled=True)]
  transfers between devices with their start and end apart: 4 -> 10, of which waited for: 4 -> 3; matrix products, arithmetic and copies ran while one was open for 7% -> 10% of each run, Pallas kernels for 0% -> 0%
where the time goes in v1:
time: 248 us; the launch traced here: 246 us
  matrix products  66.6 us (27%)
  other arithmetic  65.5 us (26%)
  waiting for transfers between devices  45.1 us (18%)
  local copies, waits for them, and re-layouts  30.7 us (12%)
  starting transfers between devices  18.5 us (7%)
  between operations  13.6 us (5%)
  blocking collectives  5.77 us (2%)
    dot_general x8, matrix products, attend(): jnp.einsum('qhck,ckl->qhl', weights, picked_values, preferred_element_typ...  35.9 us
    reduce_scatter x1, waiting for transfers between devices, own_rows(): lax.psum_scatter(everything.astype(jnp.bfloat16), axis, scatter_dimension...  30.6 us
    dot_general x8, matrix products, attend(): jnp.einsum('qhl,ckl->qhck', query_block, picked_keys, preferred_element_t...  22.3 us
    reduce_sum x8, other arithmetic, attend(): jnp.sum(exp_scores, axis=(2, 3), keepdims=True)  16.7 us
    reduce_sum x8, other arithmetic, rms_scale(): mean_sq = jnp.mean(widened * widened, axis=-1, keepdims=True)  14.7 us
    ppermute x7, starting transfers between devices, pairwise_exchange(): part = lax.ppermute(part, axis, [(d, d ^ mask) for d in range(ways)])  11.1 us
    all_gather x1, waiting for transfers between devices, taken_in(): lax.all_gather(part, axis, axis=dim, tiled=True)  9.99 us
    dynamic_update_slice x7, local copies, waits for them, and re-layouts, pairwise_exchange(): lax.dynamic_update_slice_in_dim(full, part, (here ^ mask) * height, axis=...  8.63 us
  transfers between devices with their start and end apart: 10, of which 3 were waited for; matrix products, arithmetic and copies ran while one was open for 10% of the time, Pallas kernels for 0%

profile of v1, /device:TPU:0, one launch (start us, length us, event | category | flops | bytes accessed | tf_op | source)
XLA Modules:
  0.0 246.2 jit_solution(18083606361809649599)
XLA Ops:
  10.4 7.3 %all-to-all-start = ((s32[8,1,2]{2,1,0:T(1,128)}), s32[8,1,2]{2,1,0:T(1,128)S(1)}, u32[]{:S(2)}, u32[]{:S(2)}) async-start(s32[8,1,2]{2,1,0:T(1,128)} %bitcast.27), calls=%async_computation | async-start | bytes 8192 | tf_op jit(solution)/shard_map/all_to_all | solution.py:101
  20.4 3.7 %all-to-all-done = s32[8,1,2]{2,1,0:T(1,128)S(1)} async-done(((s32[8,1,2]{2,1,0:T(1,128)}), s32[8,1,2]{2,1,0:T(1,128)S(1)}, u32[]{:S(2)}, u32[]{:S(2)}) %all-to-all-start) | async-done | bytes 96 | tf_op jit(solution)/shard_map/all_to_all | solution.py:101
  24.5 10.0 %all-gather.2.cloned.1.call-done = bf16[1024,1024]{1,0:T(8,128)(2,1)} async-done(((bf16[1024,256]{1,0:T(8,128)(2,1)}), bf16[1024,1024]{1,0:T(8,128)(2,1)}) %all-gather.2.cloned.1.call-update) | async-done | bytes 2097168 | tf_op jit(solution)/shard_map/all_gather | solution.py:29
  34.5 2.3 convolution_convert_fusion.2
  42.7 2.4 collective-permute-start.3
  46.5 3.5 %bitcast_reduce_fusion = (f32[1024,4]{0,1:T(4,128)}, bf16[1024,512]{0,1:T(8,128)(2,1)S(1)}) fusion(bf16[1024,1024]{1,0:T(8,128)(2,1)} %all-gather.2.cloned.1.call-done, bf16[1024,512]{1,0:T(8,128)(2,1)S(1)} %copy-done), kind=kOutput, calls=%fused_computation.39 | convolution fusion | flops 1075834880 | bytes 4210688 | tf_op jit(solution)/shard_map/dot_general | solution.py:69
  56.3 3.3 %collective-permute-start.5 = (bf16[1,2,128,128]{3,2,1,0:T(8,128)(2,1)S(1)}, bf16[1,2,128,128]{3,2,1,0:T(8,128)(2,1)S(1)}, u32[]{:S(2)}, u32[]{:S(2)}) collective-permute-start(bf16[1,2,128,128]{3,2,1,0:T(8,128)(2,1)S(1)} %get-tuple-element.104), channel_id=1, source_target_pairs={{0,24},{4,28},{8,16},{12,20},{16,8},{20,12},{24,0},{28,4},{1,25},{... | collective-permute-start | bytes 196616 | tf_op jit(solution)/shard_map/ppermute | solution.py:23
  69.9 8.3 %gather_fusion.2 = bf16[256,128,128]{2,1,0:T(8,128)(2,1)} fusion(bf16[24,128,128]{2,1,0:T(8,128)(2,1)S(1)} %pad_maximum_fusion, s32[1024]{0:T(1024)S(1)} %pad_clamp_fusion), kind=kCustom, calls=%fused_computation.2 | custom fusion | bytes 16778240 | tf_op jit(solution)/shard_map/gather | solution.py:112
  78.2 118.2 %while.12 = (s32[]{:T(128)}, bf16[8,128,4,128]{3,1,0,2:T(8,128)(2,1)S(1)}, s32[8,32]{1,0:T(8,128)}, s32[8]{0:T(128)S(1)}, bf16[8,128,4,128]{3,1,2,0:T(8,128)(2,1...) while((s32[]{:T(128)}, ...), condition=%wide.region_10.11_spmd.clone.clone, body=%wide.region_6.10_spmd.clone.clone.sunk | while | flops 1107893504 | bytes 30783664 | solution.py:142
  83.6 2.8 %fusion.45 = (f32[128,4]{0,1:T(4,128)S(1)}, f32[128,4,32,128]{0,3,2,1:T(8,128)S(1)}) fusion(pred[128,32,128]{0,2,1:T(8,128)(4,1)S(1)} %compare_and_fusion.3, f32[128]{0:T(128)S(1)} %get-tuple-element.187, f32[32,128]{1,0:T(8,128)S(1)} %add_rsqrt_fusion.3, bf16[8,32,128,128]{3,2,1,0:T(8,128)(2,1)} %get-tuple-element.186, s32[]{:T(128)} %get-tuple-element.173, ...), kind=kOutput, calls=%fused_computation.7.clone.1 | convolution fusion | flops 545259008 | bytes 10112512 | tf_op jit(solution)/shard_map/while/body/eval_jaxpr/qhl,ckl->qhck/dot_general | solution.py:122
  86.4 2.1 fusion.46
  88.5 4.5 %fusion.47 = bf16[8,128,4,128]{3,1,0,2:T(8,128)(2,1)S(1)} fusion(bf16[8,128,4,128]{3,1,0,2:T(8,128)(2,1)S(1)} %get-tuple-element.174, s32[]{:T(128)} %get-tuple-element.173, f32[128,4,32,128]{0,3,2,1:T(8,128)S(1)} %get-tuple-element.163, f32[128,4]{0,1:T(4,128)S(1)} %fusion.46, f32[128,4]{0,1:T(4,128)S(1)} %get-tuple-element.164, ...), kind=kOutput, calls=%fused_computation.16.clone.1 | convolution fusion | flops 549519360 | bytes 10097664 | tf_op jit(solution)/shard_map/while/body/eval_jaxpr/qhck,ckl->qhl/dot_general | solution.py:137
  98.4 2.8 %fusion.45 = (f32[128,4]{0,1:T(4,128)S(1)}, f32[128,4,32,128]{0,3,2,1:T(8,128)S(1)}) fusion(pred[128,32,128]{0,2,1:T(8,128)(4,1)S(1)} %compare_and_fusion.3, f32[128]{0:T(128)S(1)} %get-tuple-element.187, f32[32,128]{1,0:T(8,128)S(1)} %add_rsqrt_fusion.3, bf16[8,32,128,128]{3,2,1,0:T(8,128)(2,1)} %get-tuple-element.186, s32[]{:T(128)} %get-tuple-element.173, ...), kind=kOutput, calls=%fused_computation.7.clone.1 | convolution fusion | flops 545259008 | bytes 10112512 | tf_op jit(solution)/shard_map/while/body/eval_jaxpr/qhl,ckl->qhck/dot_general | solution.py:122
  101.2 2.1 fusion.46
  103.3 4.5 %fusion.47 = bf16[8,128,4,128]{3,1,0,2:T(8,128)(2,1)S(1)} fusion(bf16[8,128,4,128]{3,1,0,2:T(8,128)(2,1)S(1)} %get-tuple-element.174, s32[]{:T(128)} %get-tuple-element.173, f32[128,4,32,128]{0,3,2,1:T(8,128)S(1)} %get-tuple-element.163, f32[128,4]{0,1:T(4,128)S(1)} %fusion.46, f32[128,4]{0,1:T(4,128)S(1)} %get-tuple-element.164, ...), kind=kOutput, calls=%fused_computation.16.clone.1 | convolution fusion | flops 549519360 | bytes 10097664 | tf_op jit(solution)/shard_map/while/body/eval_jaxpr/qhck,ckl->qhl/dot_general | solution.py:137
  113.1 2.8 %fusion.45 = (f32[128,4]{0,1:T(4,128)S(1)}, f32[128,4,32,128]{0,3,2,1:T(8,128)S(1)}) fusion(pred[128,32,128]{0,2,1:T(8,128)(4,1)S(1)} %compare_and_fusion.3, f32[128]{0:T(128)S(1)} %get-tuple-element.187, f32[32,128]{1,0:T(8,128)S(1)} %add_rsqrt_fusion.3, bf16[8,32,128,128]{3,2,1,0:T(8,128)(2,1)} %get-tuple-element.186, s32[]{:T(128)} %get-tuple-element.173, ...), kind=kOutput, calls=%fused_computation.7.clone.1 | convolution fusion | flops 545259008 | bytes 10112512 | tf_op jit(solution)/shard_map/while/body/eval_jaxpr/qhl,ckl->qhck/dot_general | solution.py:122
  115.9 2.1 fusion.46
  118.0 4.5 %fusion.47 = bf16[8,128,4,128]{3,1,0,2:T(8,128)(2,1)S(1)} fusion(bf16[8,128,4,128]{3,1,0,2:T(8,128)(2,1)S(1)} %get-tuple-element.174, s32[]{:T(128)} %get-tuple-element.173, f32[128,4,32,128]{0,3,2,1:T(8,128)S(1)} %get-tuple-element.163, f32[128,4]{0,1:T(4,128)S(1)} %fusion.46, f32[128,4]{0,1:T(4,128)S(1)} %get-tuple-element.164, ...), kind=kOutput, calls=%fused_computation.16.clone.1 | convolution fusion | flops 549519360 | bytes 10097664 | tf_op jit(solution)/shard_map/while/body/eval_jaxpr/qhck,ckl->qhl/dot_general | solution.py:137
  127.9 2.8 %fusion.45 = (f32[128,4]{0,1:T(4,128)S(1)}, f32[128,4,32,128]{0,3,2,1:T(8,128)S(1)}) fusion(pred[128,32,128]{0,2,1:T(8,128)(4,1)S(1)} %compare_and_fusion.3, f32[128]{0:T(128)S(1)} %get-tuple-element.187, f32[32,128]{1,0:T(8,128)S(1)} %add_rsqrt_fusion.3, bf16[8,32,128,128]{3,2,1,0:T(8,128)(2,1)} %get-tuple-element.186, s32[]{:T(128)} %get-tuple-element.173, ...), kind=kOutput, calls=%fused_computation.7.clone.1 | convolution fusion | flops 545259008 | bytes 10112512 | tf_op jit(solution)/shard_map/while/body/eval_jaxpr/qhl,ckl->qhck/dot_general | solution.py:122
  130.7 2.1 fusion.46
  132.8 4.5 %fusion.47 = bf16[8,128,4,128]{3,1,0,2:T(8,128)(2,1)S(1)} fusion(bf16[8,128,4,128]{3,1,0,2:T(8,128)(2,1)S(1)} %get-tuple-element.174, s32[]{:T(128)} %get-tuple-element.173, f32[128,4,32,128]{0,3,2,1:T(8,128)S(1)} %get-tuple-element.163, f32[128,4]{0,1:T(4,128)S(1)} %fusion.46, f32[128,4]{0,1:T(4,128)S(1)} %get-tuple-element.164, ...), kind=kOutput, calls=%fused_computation.16.clone.1 | convolution fusion | flops 549519360 | bytes 10097664 | tf_op jit(solution)/shard_map/while/body/eval_jaxpr/qhck,ckl->qhl/dot_general | solution.py:137
  142.7 2.8 %fusion.45 = (f32[128,4]{0,1:T(4,128)S(1)}, f32[128,4,32,128]{0,3,2,1:T(8,128)S(1)}) fusion(pred[128,32,128]{0,2,1:T(8,128)(4,1)S(1)} %compare_and_fusion.3, f32[128]{0:T(128)S(1)} %get-tuple-element.187, f32[32,128]{1,0:T(8,128)S(1)} %add_rsqrt_fusion.3, bf16[8,32,128,128]{3,2,1,0:T(8,128)(2,1)} %get-tuple-element.186, s32[]{:T(128)} %get-tuple-element.173, ...), kind=kOutput, calls=%fused_computation.7.clone.1 | convolution fusion | flops 545259008 | bytes 10112512 | tf_op jit(solution)/shard_map/while/body/eval_jaxpr/qhl,ckl->qhck/dot_general | solution.py:122
  147.5 4.5 %fusion.47 = bf16[8,128,4,128]{3,1,0,2:T(8,128)(2,1)S(1)} fusion(bf16[8,128,4,128]{3,1,0,2:T(8,128)(2,1)S(1)} %get-tuple-element.174, s32[]{:T(128)} %get-tuple-element.173, f32[128,4,32,128]{0,3,2,1:T(8,128)S(1)} %get-tuple-element.163, f32[128,4]{0,1:T(4,128)S(1)} %fusion.46, f32[128,4]{0,1:T(4,128)S(1)} %get-tuple-element.164, ...), kind=kOutput, calls=%fused_computation.16.clone.1 | convolution fusion | flops 549519360 | bytes 10097664 | tf_op jit(solution)/shard_map/while/body/eval_jaxpr/qhck,ckl->qhl/dot_general | solution.py:137
  157.4 2.8 %fusion.45 = (f32[128,4]{0,1:T(4,128)S(1)}, f32[128,4,32,128]{0,3,2,1:T(8,128)S(1)}) fusion(pred[128,32,128]{0,2,1:T(8,128)(4,1)S(1)} %compare_and_fusion.3, f32[128]{0:T(128)S(1)} %get-tuple-element.187, f32[32,128]{1,0:T(8,128)S(1)} %add_rsqrt_fusion.3, bf16[8,32,128,128]{3,2,1,0:T(8,128)(2,1)} %get-tuple-element.186, s32[]{:T(128)} %get-tuple-element.173, ...), kind=kOutput, calls=%fused_computation.7.clone.1 | convolution fusion | flops 545259008 | bytes 10112512 | tf_op jit(solution)/shard_map/while/body/eval_jaxpr/qhl,ckl->qhck/dot_general | solution.py:122
  162.3 4.5 %fusion.47 = bf16[8,128,4,128]{3,1,0,2:T(8,128)(2,1)S(1)} fusion(bf16[8,128,4,128]{3,1,0,2:T(8,128)(2,1)S(1)} %get-tuple-element.174, s32[]{:T(128)} %get-tuple-element.173, f32[128,4,32,128]{0,3,2,1:T(8,128)S(1)} %get-tuple-element.163, f32[128,4]{0,1:T(4,128)S(1)} %fusion.46, f32[128,4]{0,1:T(4,128)S(1)} %get-tuple-element.164, ...), kind=kOutput, calls=%fused_computation.16.clone.1 | convolution fusion | flops 549519360 | bytes 10097664 | tf_op jit(solution)/shard_map/while/body/eval_jaxpr/qhck,ckl->qhl/dot_general | solution.py:137
  172.2 2.8 %fusion.45 = (f32[128,4]{0,1:T(4,128)S(1)}, f32[128,4,32,128]{0,3,2,1:T(8,128)S(1)}) fusion(pred[128,32,128]{0,2,1:T(8,128)(4,1)S(1)} %compare_and_fusion.3, f32[128]{0:T(128)S(1)} %get-tuple-element.187, f32[32,128]{1,0:T(8,128)S(1)} %add_rsqrt_fusion.3, bf16[8,32,128,128]{3,2,1,0:T(8,128)(2,1)} %get-tuple-element.186, s32[]{:T(128)} %get-tuple-element.173, ...), kind=kOutput, calls=%fused_computation.7.clone.1 | convolution fusion | flops 545259008 | bytes 10112512 | tf_op jit(solution)/shard_map/while/body/eval_jaxpr/qhl,ckl->qhck/dot_general | solution.py:122
  177.1 4.5 %fusion.47 = bf16[8,128,4,128]{3,1,0,2:T(8,128)(2,1)S(1)} fusion(bf16[8,128,4,128]{3,1,0,2:T(8,128)(2,1)S(1)} %get-tuple-element.174, s32[]{:T(128)} %get-tuple-element.173, f32[128,4,32,128]{0,3,2,1:T(8,128)S(1)} %get-tuple-element.163, f32[128,4]{0,1:T(4,128)S(1)} %fusion.46, f32[128,4]{0,1:T(4,128)S(1)} %get-tuple-element.164, ...), kind=kOutput, calls=%fused_computation.16.clone.1 | convolution fusion | flops 549519360 | bytes 10097664 | tf_op jit(solution)/shard_map/while/body/eval_jaxpr/qhck,ckl->qhl/dot_general | solution.py:137
  186.9 2.8 %fusion.45 = (f32[128,4]{0,1:T(4,128)S(1)}, f32[128,4,32,128]{0,3,2,1:T(8,128)S(1)}) fusion(pred[128,32,128]{0,2,1:T(8,128)(4,1)S(1)} %compare_and_fusion.3, f32[128]{0:T(128)S(1)} %get-tuple-element.187, f32[32,128]{1,0:T(8,128)S(1)} %add_rsqrt_fusion.3, bf16[8,32,128,128]{3,2,1,0:T(8,128)(2,1)} %get-tuple-element.186, s32[]{:T(128)} %get-tuple-element.173, ...), kind=kOutput, calls=%fused_computation.7.clone.1 | convolution fusion | flops 545259008 | bytes 10112512 | tf_op jit(solution)/shard_map/while/body/eval_jaxpr/qhl,ckl->qhck/dot_general | solution.py:122
  191.8 4.5 %fusion.47 = bf16[8,128,4,128]{3,1,0,2:T(8,128)(2,1)S(1)} fusion(bf16[8,128,4,128]{3,1,0,2:T(8,128)(2,1)S(1)} %get-tuple-element.174, s32[]{:T(128)} %get-tuple-element.173, f32[128,4,32,128]{0,3,2,1:T(8,128)S(1)} %get-tuple-element.163, f32[128,4]{0,1:T(4,128)S(1)} %fusion.46, f32[128,4]{0,1:T(4,128)S(1)} %get-tuple-element.164, ...), kind=kOutput, calls=%fused_computation.16.clone.1 | convolution fusion | flops 549519360 | bytes 10097664 | tf_op jit(solution)/shard_map/while/body/eval_jaxpr/qhck,ckl->qhl/dot_general | solution.py:137
  196.8 2.1 convert_bitcast_fusion.1
  199.7 30.6 %reduce-scatter.2.cloned.1.call-done = bf16[256,1024]{0,1:T(8,128)(2,1)} async-done(((bf16[1024,1024]{0,1:T(8,128)(2,1)}), bf16[256,1024]{0,1:T(8,128)(2,1)}) %reduce-scatter.2.cloned.1.call-update) | async-done | bytes 524304 | tf_op jit(solution)/shard_map/reduce_scatter | solution.py:35
  231.6 5.8 %psum.7 = f32[1024]{0:T(1024)S(1)} all-reduce(f32[1024]{0:T(1024)S(1)} %fusion.24), channel_id=1, replica_groups=mesh['kv'=8,'tp'=4] {'tp'}, use_global_device_ids=true, to_apply=%region_13.14 | all-reduce | flops 1024 | bytes 8192 | tf_op jit(solution)/shard_map/psum | solution.py:160
  (149 shorter events, 86.2 us)
Async XLA Ops:
  6.5 40.0 %copy-start = (bf16[1024,512]{1,0:T(8,128)(2,1)S(1)}, bf16[1024,512]{1,0:T(8,128)(2,1)}, u32[]{:S(2)}) copy-start(bf16[1024,512]{1,0:T(8,128)(2,1)} %param.12) | copy-start | bytes 3145732
  6.5 27.9 %all-gather.2.cloned.1.call-start = ((), (), s32[]{:S(2)}) async-start(), calls=%async_computation.2 | async-start | bytes 2621440 | tf_op jit(solution)/shard_map/all_gather | solution.py:29
  10.4 13.7 %all-to-all-start = ((s32[8,1,2]{2,1,0:T(1,128)}), s32[8,1,2]{2,1,0:T(1,128)S(1)}, u32[]{:S(2)}, u32[]{:S(2)}) async-start(s32[8,1,2]{2,1,0:T(1,128)} %bitcast.27), calls=%async_computation | async-start | bytes 8192 | tf_op jit(solution)/shard_map/all_to_all | solution.py:101
  17.7 212.6 %reduce-scatter.2.cloned.1.call-start = ((), (), s32[]{:S(2)}) async-start(), calls=%async_computation.3 | async-start | bytes 2621440 | tf_op jit(solution)/shard_map/reduce_scatter | solution.py:35
  39.2 17.1 %collective-permute-start = (bf16[1,2,128,128]{3,2,1,0:T(8,128)(2,1)}, bf16[1,2,128,128]{3,2,1,0:T(8,128)(2,1)}, u32[]{:S(2)}, u32[]{:S(2)}) collective-permute-start(bf16[1,2,128,128]{3,2,1,0:T(8,128)(2,1)} %get-tuple-element.109), channel_id=1, source_target_pairs={{0,4},{4,0},{8,12},{12,8},{16,20},{20,16},{24,28},{28,24},{1,5},{5... | collective-permute-start | bytes 196616 | tf_op jit(solution)/shard_map/ppermute | solution.py:23
  40.6 20.4 %collective-permute-start.1 = (bf16[1,2,128,128]{3,2,1,0:T(8,128)(2,1)}, bf16[1,2,128,128]{3,2,1,0:T(8,128)(2,1)}, u32[]{:S(2)}, u32[]{:S(2)}) collective-permute-start(bf16[1,2,128,128]{3,2,1,0:T(8,128)(2,1)} %get-tuple-element.108), channel_id=1, source_target_pairs={{0,8},{4,12},{8,0},{12,4},{16,24},{20,28},{24,16},{28,20},{1,9},{5... | collective-permute-start | bytes 196616 | tf_op jit(solution)/shard_map/ppermute | solution.py:23
  42.1 20.9 %collective-permute-start.2 = (bf16[1,2,128,128]{3,2,1,0:T(8,128)(2,1)}, bf16[1,2,128,128]{3,2,1,0:T(8,128)(2,1)}, u32[]{:S(2)}, u32[]{:S(2)}) collective-permute-start(bf16[1,2,128,128]{3,2,1,0:T(8,128)(2,1)} %get-tuple-element.107), channel_id=1, source_target_pairs={{0,12},{4,8},{8,4},{12,0},{16,28},{20,24},{24,20},{28,16},{1,13},{... | collective-permute-start | bytes 196616 | tf_op jit(solution)/shard_map/ppermute | solution.py:23
  42.7 21.8 %collective-permute-start.3 = (bf16[1,2,128,128]{3,2,1,0:T(8,128)(2,1)}, bf16[1,2,128,128]{3,2,1,0:T(8,128)(2,1)}, u32[]{:S(2)}, u32[]{:S(2)}) collective-permute-start(bf16[1,2,128,128]{3,2,1,0:T(8,128)(2,1)} %get-tuple-element.106), channel_id=1, source_target_pairs={{0,16},{4,20},{8,24},{12,28},{16,0},{20,4},{24,8},{28,12},{1,17},{... | collective-permute-start | bytes 196616 | tf_op jit(solution)/shard_map/ppermute | solution.py:23
  45.1 9.7 %copy-start.4 = (f32[128]{0:T(128)S(1)}, f32[128]{0:T(128)}, u32[]{:S(2)}) copy-start(f32[128]{0:T(128)} %param.14) | copy-start | bytes 1540
  45.1 20.9 %collective-permute-start.4 = (bf16[1,2,128,128]{3,2,1,0:T(8,128)(2,1)}, bf16[1,2,128,128]{3,2,1,0:T(8,128)(2,1)}, u32[]{:S(2)}, u32[]{:S(2)}) collective-permute-start(bf16[1,2,128,128]{3,2,1,0:T(8,128)(2,1)} %get-tuple-element.105), channel_id=1, source_target_pairs={{0,20},{4,16},{8,28},{12,24},{16,4},{20,0},{24,12},{28,8},{1,21},{... | collective-permute-start | bytes 196616 | tf_op jit(solution)/shard_map/ppermute | solution.py:23
  56.3 11.2 %collective-permute-start.5 = (bf16[1,2,128,128]{3,2,1,0:T(8,128)(2,1)S(1)}, bf16[1,2,128,128]{3,2,1,0:T(8,128)(2,1)S(1)}, u32[]{:S(2)}, u32[]{:S(2)}) collective-permute-start(bf16[1,2,128,128]{3,2,1,0:T(8,128)(2,1)S(1)} %get-tuple-element.104), channel_id=1, source_target_pairs={{0,24},{4,28},{8,16},{12,20},{16,8},{20,12},{24,0},{28,4},{1,25},{... | collective-permute-start | bytes 196616 | tf_op jit(solution)/shard_map/ppermute | solution.py:23
  61.1 7.0 %collective-permute-start.6 = (bf16[1,2,128,128]{3,2,1,0:T(8,128)(2,1)S(1)}, bf16[1,2,128,128]{3,2,1,0:T(8,128)(2,1)S(1)}, u32[]{:S(2)}, u32[]{:S(2)}) collective-permute-start(bf16[1,2,128,128]{3,2,1,0:T(8,128)(2,1)S(1)} %get-tuple-element.103), channel_id=1, source_target_pairs={{0,28},{4,24},{8,20},{12,16},{16,12},{20,8},{24,4},{28,0},{1,29},{... | collective-permute-start | bytes 196616 | tf_op jit(solution)/shard_map/ppermute | solution.py:23
  69.8 8.3 %copy-start.1 = (bf16[8,128,4,128]{3,1,0,2:T(8,128)(2,1)S(1)}, bf16[8,128,4,128]{3,1,0,2:T(8,128)(2,1)}, u32[]{:S(2)}) copy-start(bf16[8,128,4,128]{3,1,0,2:T(8,128)(2,1)} %custom-call.6) | copy-start | bytes 3145732
  69.8 8.3 %copy-start.5 = (f32[128]{0:T(128)S(1)}, f32[128]{0:T(128)}, u32[]{:S(2)}) copy-start(f32[128]{0:T(128)} %param.15) | copy-start | bytes 1540
  78.2 118.2 %copy-start.3 = (bf16[4,128,64]{1,2,0:T(8,128)(2,1)S(1)}, bf16[4,128,64]{1,2,0:T(8,128)(2,1)}, u32[]{:S(2)}) copy-start(bf16[4,128,64]{1,2,0:T(8,128)(2,1)} %param.16) | copy-start | bytes 196612
  78.2 118.7 %copy-start.2 = (bf16[256,1024]{1,0:T(8,128)(2,1)S(1)}, bf16[256,1024]{1,0:T(8,128)(2,1)}, u32[]{:S(2)}) copy-start(bf16[256,1024]{1,0:T(8,128)(2,1)} %param.17) | copy-start | bytes 1572868
Sparse Core Ops, SparseCore 0:
  8.9 25.5 all-gather.1
  199.1 31.1 reduce-scatter.1
